TPU v7x, 32 devices: a whole 2x2x4 slice. The times are simulated.
32 devices in a mesh: sp: 8 (over z, x), tp: 4 (over y, core).
Axes of the slice: x: 2, y: 2, z: 4, core: 2. Of those that a mesh axis runs over, the one named last changes fastest.
Arguments:
- latent: bfloat16 [6144, 2048], P(('sp', 'tp')), may hold values from -6 to 6
- context: bfloat16 [1024, 2048], P('sp'), may hold values from -6 to 6
- conditioning: float32 [2, 2048], replicated, may hold values from -6 to 6
- norm_gain: float32 [2048], replicated, may hold values from 0.1 to 1.9
- mod_shift: bfloat16 [2048, 2048], P('sp', 'tp'), may hold values from -0.1875 to 0.1875
- mod_scale: bfloat16 [2048, 2048], P('sp', 'tp'), may hold values from -0.1875 to 0.1875
- mod_gate: bfloat16 [2048, 2048], P('sp', 'tp'), may hold values from -0.1875 to 0.1875
- w_query: bfloat16 [2048, 2048], P(None, 'tp'), may hold values from -4 to 4
- w_key: bfloat16 [2048, 2048], P(None, 'tp'), may hold values from -0.125 to 0.125
- w_value: bfloat16 [2048, 2048], P(None, 'tp'), may hold values from -0.125 to 0.125
- w_out: bfloat16 [2048, 2048], P('tp'), may hold values from -0.125 to 0.125
- lambdas: float32 [16], P('tp'), may hold values from 0.3 to 0.8
- context_bias: float32 [16], P('tp'), may hold values from 0.8 to 2.2
- head_gain: float32 [128], replicated, may hold values from 0.1 to 1.9
Outputs:
- updated: bfloat16 [6144, 2048], P(('sp', 'tp'))
All inputs are finite; a program needn't handle non-finite values.
Results may differ from a plain program's by a relative error of at most 0.01.
The roundings to bfloat16 on the way count: a program that leaves them out, or rounds other values in their place, can miss the bound.
Values may be sent and summed in bfloat16 or wider, within the bound.
A program may use at most 128 MiB of HBM per device.

v0:
```python
import jax
import jax.numpy as jnp
from jax import lax
from jax.sharding import PartitionSpec as P

EPS = 1e-06
NEGATIVE = -1e30


def modulated(inputs, norm_scale, offset_vec, scale_vec):
    rows_float = inputs.astype(jnp.float32)
    normal = rows_float * lax.rsqrt(jnp.mean(rows_float * rows_float, axis=-1, keepdims=True) + EPS)
    return (normal * norm_scale * (1.0 + scale_vec) + offset_vec).astype(jnp.bfloat16)


def block_size(length):
    for candidate in range(min(length, 1024), 0, -1):
        if length % candidate == 0:
            return candidate
    return length


def absorb(running, portion, context_flags, queries, bias_heads):
    head_count = queries.shape[1]
    head_dim = queries.shape[3]
    row_count = portion.shape[0]
    head_cols = head_count * 2 * head_dim
    key_rows = portion[:, :head_cols].reshape(row_count, head_count, 2, head_dim)
    value_rows = portion[:, head_cols:].reshape(row_count, head_count, 2 * head_dim)
    shifts = bias_heads[:, None, None] * context_flags[None, None, :]
    updated = []
    for which_map in range(2):
        previous, weight, accumulated = running[3 * which_map : 3 * which_map + 3]
        scores = (
            jnp.einsum(
                "qhd,khd->hqk",
                queries[:, :, which_map],
                key_rows[:, :, which_map],
                preferred_element_type=jnp.float32,
            )
            * head_dim ** (-0.5)
            + shifts
        )
        peak_new = jnp.maximum(previous, jnp.max(scores, axis=2))
        faded = jnp.exp(previous - peak_new)
        raised = jnp.exp(scores - peak_new[:, :, None])
        weight = weight * faded + jnp.sum(raised, axis=2)
        accumulated = accumulated * faded.T[:, :, None] + jnp.einsum(
            "hqk,khd->qhd",
            raised.astype(jnp.bfloat16),
            value_rows,
            preferred_element_type=jnp.float32,
        )
        updated += [peak_new, weight, accumulated]
    return tuple(updated)


def absorb_rows(running, portion, context_flags, queries, bias_heads):
    row_count = portion.shape[0]
    block_len = block_size(row_count)
    if block_len == row_count:
        return absorb(running, portion, context_flags, queries, bias_heads)
    stacked = portion.reshape(row_count // block_len, block_len, portion.shape[1])
    flag_blocks = context_flags.reshape(row_count // block_len, block_len)

    def advance(state_now, operand):
        return (absorb(state_now, operand[0], operand[1], queries, bias_heads), None)

    running, unused = lax.scan(advance, running, (stacked, flag_blocks))
    return running


def per_device(
    latent,
    context,
    conditioning,
    norm_gain,
    mod_shift,
    mod_scale,
    mod_gate,
    w_query,
    w_key,
    w_value,
    w_out,
    lambdas,
    context_bias,
    head_gain,
):
    head_dim = head_gain.shape[0] // 2
    head_count = lambdas.shape[0]
    rows_sp = mod_shift.shape[0]
    cond_rows = lax.dynamic_slice_in_dim(conditioning, lax.axis_index("sp") * rows_sp, rows_sp, 1)
    activated = jax.nn.silu(cond_rows).astype(jnp.bfloat16)
    partials = jnp.stack(
        [
            jnp.dot(activated, matrix, preferred_element_type=jnp.float32)
            for matrix in (mod_shift, mod_scale, mod_gate)
        ],
        axis=1,
    )
    summed = lax.psum(partials, "sp")
    modulation = lax.all_gather(summed, "tp", axis=2, tiled=True)
    own_rows = modulated(latent, norm_gain, modulation[0, 0], modulation[0, 1])
    context_rows = modulated(context, norm_gain, modulation[1, 0], modulation[1, 1])
    key_value = jnp.concatenate([w_key, w_value], axis=1)
    projector = jnp.concatenate([w_query, key_value], axis=1)
    projected = jnp.dot(
        lax.all_gather(own_rows, "tp", axis=0, tiled=True),
        projector,
        preferred_element_type=jnp.float32,
    ).astype(jnp.bfloat16)
    head_cols = w_query.shape[1]
    token_count = projected.shape[0]
    queries = projected[:, :head_cols].reshape(token_count, head_count, 2, head_dim)
    latent_kv = projected[:, head_cols:]
    context_kv = jnp.dot(context_rows, key_value, preferred_element_type=jnp.float32).astype(
        jnp.bfloat16
    )
    first_map = (
        jnp.full((head_count, token_count), NEGATIVE, jnp.float32),
        jnp.zeros((head_count, token_count), jnp.float32),
        jnp.zeros((token_count, head_count, 2 * head_dim), jnp.float32),
    )
    initial = first_map + first_map
    every_context = lax.all_gather(context_kv, "sp", axis=0, tiled=True)
    running = absorb_rows(
        initial,
        every_context,
        jnp.ones((every_context.shape[0],), jnp.float32),
        queries,
        context_bias,
    )
    portion = lax.all_gather(latent_kv, "sp", axis=0, tiled=True)
    running = absorb_rows(
        running, portion, jnp.zeros((portion.shape[0],), jnp.float32), queries, context_bias
    )
    peak_one, total_one, accum_one, peak_two, total_two, accum_two = running
    mixed = accum_one / total_one.T[:, :, None] - lambdas[None, :, None] * (
        accum_two / total_two.T[:, :, None]
    )
    normed = mixed * lax.rsqrt(jnp.mean(mixed * mixed, axis=-1, keepdims=True) + EPS) * head_gain
    flattened = normed.reshape(token_count, head_cols).astype(jnp.bfloat16)
    attended = lax.psum_scatter(
        jnp.dot(flattened, w_out, preferred_element_type=jnp.float32).astype(jnp.bfloat16),
        "tp",
        scatter_dimension=0,
        tiled=True,
    )
    return (latent.astype(jnp.float32) + modulation[0, 2] * attended.astype(jnp.float32)).astype(
        jnp.bfloat16
    )


def solution(mesh):
    return jax.shard_map(
        per_device,
        mesh=mesh,
        in_specs=(
            P(("sp", "tp"), None),
            P("sp", None),
            P(),
            P(),
            P("sp", "tp"),
            P("sp", "tp"),
            P("sp", "tp"),
            P(None, "tp"),
            P(None, "tp"),
            P(None, "tp"),
            P("tp", None),
            P("tp"),
            P("tp"),
            P(),
        ),
        out_specs=P(("sp", "tp"), None),
        check_vma=False,
    )
```

profile of v0, /device:TPU:0, one launch (start us, length us, event | category | flops | bytes accessed | tf_op | source)
XLA Modules:
  0.0 557.7 jit_solution(13907041467783386179)
XLA Ops:
  10.0 38.8 %psum.7 = f32[2,3,512]{2,0,1:T(2,128)S(1)} all-reduce(f32[2,3,512]{2,0,1:T(2,128)S(1)} %pad_maximum_fusion), channel_id=1, replica_groups=mesh['sp'=8,'tp'=4] {'sp'}, use_global_device_ids=true, to_apply=%region_0.1 | all-reduce | flops 3072 | bytes 24576 | tf_op jit(solution)/shard_map/psum | solution.py:101
  48.9 5.2 all_gather.12
  59.8 4.0 fusion.57
  63.9 20.6 %all-gather.4.cloned.1.call-done = bf16[768,2048]{1,0:T(8,128)(2,1)} async-done(((bf16[192,2048]{1,0:T(8,128)(2,1)}), bf16[768,2048]{1,0:T(8,128)(2,1)}) %all-gather.4.cloned.1.call-update) | async-done | bytes 3145744 | tf_op jit(solution)/shard_map/all_gather | solution.py:108
  84.5 8.8 %fusion.44 = bf16[768,1536]{1,0:T(8,128)(2,1)S(1)} fusion(bf16[768,2048]{1,0:T(8,128)(2,1)} %all-gather.4.cloned.1.call-done, bf16[2048,512]{1,0:T(8,128)(2,1)} %param.25, bf16[2048,512]{1,0:T(8,128)(2,1)} %param.24, bf16[2048,512]{1,0:T(8,128)(2,1)} %param.23), kind=kOutput, calls=%fused_computation.56 | convolution fusion | flops 4851892224 | bytes 11796480 | tf_op jit(solution)/shard_map/dot_general | solution.py:107
  96.4 39.3 %all-gather.6.cloned.1.call-done = bf16[1024,1024]{1,0:T(8,128)(2,1)} async-done(((bf16[128,1024]{1,0:T(8,128)(2,1)}), bf16[1024,1024]{1,0:T(8,128)(2,1)}) %all-gather.6.cloned.1.call-update) | async-done | bytes 2097168 | tf_op jit(solution)/shard_map/all_gather | solution.py:125
  135.7 2.7 fusion.85
  146.5 3.1 fusion.67
  149.7 6.2 %fusion.25 = (f32[4,768]{1,0:T(4,128)S(1)}, f32[4,768]{1,0:T(4,128)S(1)}, f32[4,768,1024]{2,1,0:T(8,128)}) fusion(f32[4]{0:T(128)S(1)} %copy-done.9, f32[4,768,1024]{2,1,0:T(8,128)S(1)} %fusion.67, bf16[1024,4,2,64]{0,3,2,1:T(8,128)(2,1)S(1)} %bitcast.155, bf16[768,4,2,64]{0,3,2,1:T(8,128)(2,1)S(1)} %bitcast.153), kind=kOutput, calls=%fused_computation.39 | convolution fusion | flops 421521408 | bytes 26108416 | tf_op jit(solution)/shard_map/qhd,khd->hqk/dot_general | solution.py:35
  155.8 8.2 %fusion.29 = (f32[4,768]{1,0:T(4,128)S(1)}, f32[4,768]{1,0:T(4,128)S(1)}) fusion(f32[4,768,1024]{2,1,0:T(8,128)} %get-tuple-element.134, f32[4,768]{1,0:T(4,128)S(1)} %broadcast_maximum_fusion, f32[4]{0:T(128)S(1)} %copy-done.9, f32[4,768]{1,0:T(4,128)S(1)} %broadcast_maximum_fusion.1, f32[4,768,1024]{2,1,0:T(8,128)S(1)} %fusion.67), kind=kLoop, calls=%fused_computation.43 | loop fusion | flops 25159680 | bytes 25214992 | tf_op jit(solution)/shard_map/reduce_sum | solution.py:47
  164.0 8.6 %bitcast_add_fusion.2 = f32[768,4,128]{0,2,1:T(8,128)} fusion(bf16[1024,4,128]{0,2,1:T(8,128)(2,1)S(1)} %bitcast.156, f32[4,768,1024]{2,1,0:T(8,128)} %get-tuple-element.134, f32[4,768]{1,0:T(4,128)S(1)} %broadcast_maximum_fusion, f32[4]{0:T(128)S(1)} %copy-done.9, f32[768,4]{0,1:T(4,128)S(1)} %get-tuple-element.136), kind=kOutput, calls=%fused_computation.67 | convolution fusion | flops 818282496 | bytes 15228944 | tf_op jit(solution)/shard_map/hqk,khd->qhd/dot_general | solution.py:48
  172.7 4.1 bitcast_add_fusion.3
  176.8 135.7 %all-gather.8.cloned.1.call-done = bf16[6144,1024]{1,0:T(8,128)(2,1)} async-done(((bf16[768,1024]{1,0:T(8,128)(2,1)}), bf16[6144,1024]{1,0:T(8,128)(2,1)}) %all-gather.8.cloned.1.call-update) | async-done | bytes 12582928 | tf_op jit(solution)/shard_map/all_gather | solution.py:133
  312.6 193.9 %while.20 = (s32[]{:T(128)}, f32[4,768]{1,0:T(4,128)S(1)}, f32[4,768]{1,0:T(4,128)S(1)}, f32[768,4,128]{0,2,1:T(8,128)}, f32[4,768]{1,0:T(4,128)S(1)}, /*index=5...) while((s32[]{:T(128)}, f32[4,768]{1,0:T(4,128)S(1)}, ...), condition=%wide.region_12.13_spmd, body=%wide.region_7.12_spmd.sunk | while | flops 2486716416 | bytes 128058136 | solution.py:69
  312.6 3.1 constant_dynamic-slice_fusion.2
  315.7 3.9 copy.54
  319.6 2.7 fusion.114
  322.3 2.8 fusion.115
  325.1 5.5 bitcast_reduce_fusion.3
  330.7 5.8 %bitcast_add_fusion.7 = f32[768,4,128]{0,2,1:T(8,128)} fusion(f32[768,4,128]{0,2,1:T(8,128)} %get-tuple-element.241, bf16[1024,4,128]{0,2,1:T(8,128)(2,1)} %bitcast.148, f32[4,1024,768]{2,1,0:T(8,128)S(1)} %get-tuple-element.214, f32[4,768]{1,0:T(4,128)S(1)} %get-tuple-element.250, f32[4]{0:T(128)S(1)} %broadcast_multiply_fusion.2, ...), kind=kOutput, calls=%fused_computation.14.clone.1 | convolution fusion | flops 818675712 | bytes 16801808 | tf_op jit(solution)/shard_map/while/body/eval_jaxpr/hqk,khd->qhd/dot_general | solution.py:48
  336.5 3.2 bitcast_add_fusion.6
  339.7 5.1 fusion.118
  344.9 3.1 constant_dynamic-slice_fusion.2
  348.0 3.9 copy.54
  351.9 2.7 fusion.114
  354.6 2.8 fusion.115
  357.5 5.5 bitcast_reduce_fusion.3
  363.0 5.8 %bitcast_add_fusion.7 = f32[768,4,128]{0,2,1:T(8,128)} fusion(f32[768,4,128]{0,2,1:T(8,128)} %get-tuple-element.241, bf16[1024,4,128]{0,2,1:T(8,128)(2,1)} %bitcast.148, f32[4,1024,768]{2,1,0:T(8,128)S(1)} %get-tuple-element.214, f32[4,768]{1,0:T(4,128)S(1)} %get-tuple-element.250, f32[4]{0:T(128)S(1)} %broadcast_multiply_fusion.2, ...), kind=kOutput, calls=%fused_computation.14.clone.1 | convolution fusion | flops 818675712 | bytes 16801808 | tf_op jit(solution)/shard_map/while/body/eval_jaxpr/hqk,khd->qhd/dot_general | solution.py:48
  368.8 3.2 bitcast_add_fusion.6
  372.0 5.1 fusion.118
  377.2 3.1 constant_dynamic-slice_fusion.2
  380.3 3.9 copy.54
  384.2 2.7 fusion.114
  386.9 2.8 fusion.115
  389.8 5.5 bitcast_reduce_fusion.3
  395.3 5.8 %bitcast_add_fusion.7 = f32[768,4,128]{0,2,1:T(8,128)} fusion(f32[768,4,128]{0,2,1:T(8,128)} %get-tuple-element.241, bf16[1024,4,128]{0,2,1:T(8,128)(2,1)} %bitcast.148, f32[4,1024,768]{2,1,0:T(8,128)S(1)} %get-tuple-element.214, f32[4,768]{1,0:T(4,128)S(1)} %get-tuple-element.250, f32[4]{0:T(128)S(1)} %broadcast_multiply_fusion.2, ...), kind=kOutput, calls=%fused_computation.14.clone.1 | convolution fusion | flops 818675712 | bytes 16801808 | tf_op jit(solution)/shard_map/while/body/eval_jaxpr/hqk,khd->qhd/dot_general | solution.py:48
  401.1 3.2 bitcast_add_fusion.6
  404.3 5.1 fusion.118
  409.5 3.1 constant_dynamic-slice_fusion.2
  412.6 3.9 copy.54
  416.6 2.7 fusion.114
  419.3 2.8 fusion.115
  422.1 5.5 bitcast_reduce_fusion.3
  427.6 5.8 %bitcast_add_fusion.7 = f32[768,4,128]{0,2,1:T(8,128)} fusion(f32[768,4,128]{0,2,1:T(8,128)} %get-tuple-element.241, bf16[1024,4,128]{0,2,1:T(8,128)(2,1)} %bitcast.148, f32[4,1024,768]{2,1,0:T(8,128)S(1)} %get-tuple-element.214, f32[4,768]{1,0:T(4,128)S(1)} %get-tuple-element.250, f32[4]{0:T(128)S(1)} %broadcast_multiply_fusion.2, ...), kind=kOutput, calls=%fused_computation.14.clone.1 | convolution fusion | flops 818675712 | bytes 16801808 | tf_op jit(solution)/shard_map/while/body/eval_jaxpr/hqk,khd->qhd/dot_general | solution.py:48
  433.4 3.2 bitcast_add_fusion.6
  436.6 5.1 fusion.118
  441.9 3.1 constant_dynamic-slice_fusion.2
  445.0 3.9 copy.54
  448.9 2.7 fusion.114
  451.6 2.8 fusion.115
  454.4 5.5 bitcast_reduce_fusion.3
  459.9 5.8 %bitcast_add_fusion.7 = f32[768,4,128]{0,2,1:T(8,128)} fusion(f32[768,4,128]{0,2,1:T(8,128)} %get-tuple-element.241, bf16[1024,4,128]{0,2,1:T(8,128)(2,1)} %bitcast.148, f32[4,1024,768]{2,1,0:T(8,128)S(1)} %get-tuple-element.214, f32[4,768]{1,0:T(4,128)S(1)} %get-tuple-element.250, f32[4]{0:T(128)S(1)} %broadcast_multiply_fusion.2, ...), kind=kOutput, calls=%fused_computation.14.clone.1 | convolution fusion | flops 818675712 | bytes 16801808 | tf_op jit(solution)/shard_map/while/body/eval_jaxpr/hqk,khd->qhd/dot_general | solution.py:48
  465.7 3.2 bitcast_add_fusion.6
  469.0 5.1 fusion.118
  474.2 3.1 constant_dynamic-slice_fusion.2
  477.3 3.9 copy.54
  481.2 2.7 fusion.114
  483.9 2.8 fusion.115
  486.7 5.5 bitcast_reduce_fusion.3
  492.3 5.8 %bitcast_add_fusion.7 = f32[768,4,128]{0,2,1:T(8,128)} fusion(f32[768,4,128]{0,2,1:T(8,128)} %get-tuple-element.241, bf16[1024,4,128]{0,2,1:T(8,128)(2,1)} %bitcast.148, f32[4,1024,768]{2,1,0:T(8,128)S(1)} %get-tuple-element.214, f32[4,768]{1,0:T(4,128)S(1)} %get-tuple-element.250, f32[4]{0:T(128)S(1)} %broadcast_multiply_fusion.2, ...), kind=kOutput, calls=%fused_computation.14.clone.1 | convolution fusion | flops 818675712 | bytes 16801808 | tf_op jit(solution)/shard_map/while/body/eval_jaxpr/hqk,khd->qhd/dot_general | solution.py:48
  498.1 3.2 bitcast_add_fusion.6
  501.3 5.1 fusion.118
  509.1 3.5 convolution_convert_fusion
  512.7 36.2 %reduce-scatter.2.cloned.1.call-done = bf16[192,2048]{1,0:T(8,128)(2,1)} async-done(((bf16[768,2048]{1,0:T(8,128)(2,1)}), bf16[192,2048]{1,0:T(8,128)(2,1)}) %reduce-scatter.2.cloned.1.call-update) | async-done | bytes 786448 | tf_op jit(solution)/shard_map/reduce_scatter | solution.py:143
  (121 shorter events, 26.0 us)
Async XLA Ops:
  6.5 502.6 %copy-start = (bf16[512,2048]{1,0:T(8,128)(2,1)S(1)}, bf16[512,2048]{1,0:T(8,128)(2,1)}, u32[]{:S(2)}) copy-start(bf16[512,2048]{1,0:T(8,128)(2,1)} %param.26) | copy-start | bytes 6291460
  6.5 77.9 %all-gather.4.cloned.1.call-start = ((), (), s32[]{:S(2)}) async-start(), calls=%async_computation.1 | async-start | bytes 3932160 | tf_op jit(solution)/shard_map/all_gather | solution.py:108
  58.5 77.2 %all-gather.6.cloned.1.call-start = ((), (), s32[]{:S(2)}) async-start(), calls=%async_computation.2 | async-start | bytes 2359296 | tf_op jit(solution)/shard_map/all_gather | solution.py:125
  63.8 248.7 %all-gather.8.cloned.1.call-start = ((), (), s32[]{:S(2)}) async-start(), calls=%async_computation.3 | async-start | bytes 14155776 | tf_op jit(solution)/shard_map/all_gather | solution.py:133
  93.2 1.4 copy-start.4
  96.2 452.7 %reduce-scatter.2.cloned.1.call-start = ((), (), s32[]{:S(2)}) async-start(), calls=%async_computation.4 | async-start | bytes 3932160 | tf_op jit(solution)/shard_map/reduce_scatter | solution.py:143
  146.5 3.1 copy-start.3
  146.5 3.1 copy-start.9
  155.8 8.2 %copy-start.7 = (bf16[1024,512]{0,1:T(8,128)(2,1)S(1)}, bf16[1024,512]{0,1:T(8,128)(2,1)}, u32[]{:S(2)}) copy-start(bf16[1024,512]{0,1:T(8,128)(2,1)} %copy.41) | copy-start | bytes 3145732
  312.6 193.9 %copy-start.10 = (f32[4]{0:T(128)S(1)}, f32[4]{0:T(128)}, u32[]{:S(2)}) copy-start(f32[4]{0:T(128)} %param.27) | copy-start | bytes 52
  312.6 196.2 %copy-start.11 = (f32[128]{0:T(128)S(1)}, f32[128]{0:T(128)}, u32[]{:S(2)}) copy-start(f32[128]{0:T(128)} %param.29) | copy-start | bytes 1540
  330.6 5.8 %copy-start.1 = (bf16[1024,512]{0,1:T(8,128)(2,1)S(1)}, bf16[1024,512]{0,1:T(8,128)(2,1)}, u32[]{:S(2)}) copy-start(bf16[1024,512]{0,1:T(8,128)(2,1)} %get-tuple-element.220) | copy-start | bytes 3145732 | tf_op jit(solution)/shard_map/while
  330.6 5.8 %copy-start.5 = (f32[768,4,128]{0,2,1:T(8,128)S(1)}, f32[768,4,128]{0,2,1:T(8,128)}, u32[]{:S(2)}) copy-start(f32[768,4,128]{0,2,1:T(8,128)} %get-tuple-element.238) | copy-start | bytes 4718596 | tf_op jit(solution)/shard_map/while
  339.7 5.2 copy-start.6
  363.0 5.8 %copy-start.1 = (bf16[1024,512]{0,1:T(8,128)(2,1)S(1)}, bf16[1024,512]{0,1:T(8,128)(2,1)}, u32[]{:S(2)}) copy-start(bf16[1024,512]{0,1:T(8,128)(2,1)} %get-tuple-element.220) | copy-start | bytes 3145732 | tf_op jit(solution)/shard_map/while
  363.0 5.8 %copy-start.5 = (f32[768,4,128]{0,2,1:T(8,128)S(1)}, f32[768,4,128]{0,2,1:T(8,128)}, u32[]{:S(2)}) copy-start(f32[768,4,128]{0,2,1:T(8,128)} %get-tuple-element.238) | copy-start | bytes 4718596 | tf_op jit(solution)/shard_map/while
  372.0 5.2 copy-start.6
  395.3 5.8 %copy-start.1 = (bf16[1024,512]{0,1:T(8,128)(2,1)S(1)}, bf16[1024,512]{0,1:T(8,128)(2,1)}, u32[]{:S(2)}) copy-start(bf16[1024,512]{0,1:T(8,128)(2,1)} %get-tuple-element.220) | copy-start | bytes 3145732 | tf_op jit(solution)/shard_map/while
  395.3 5.8 %copy-start.5 = (f32[768,4,128]{0,2,1:T(8,128)S(1)}, f32[768,4,128]{0,2,1:T(8,128)}, u32[]{:S(2)}) copy-start(f32[768,4,128]{0,2,1:T(8,128)} %get-tuple-element.238) | copy-start | bytes 4718596 | tf_op jit(solution)/shard_map/while
  404.3 5.2 copy-start.6
  427.6 5.8 %copy-start.1 = (bf16[1024,512]{0,1:T(8,128)(2,1)S(1)}, bf16[1024,512]{0,1:T(8,128)(2,1)}, u32[]{:S(2)}) copy-start(bf16[1024,512]{0,1:T(8,128)(2,1)} %get-tuple-element.220) | copy-start | bytes 3145732 | tf_op jit(solution)/shard_map/while
  427.6 5.8 %copy-start.5 = (f32[768,4,128]{0,2,1:T(8,128)S(1)}, f32[768,4,128]{0,2,1:T(8,128)}, u32[]{:S(2)}) copy-start(f32[768,4,128]{0,2,1:T(8,128)} %get-tuple-element.238) | copy-start | bytes 4718596 | tf_op jit(solution)/shard_map/while
  436.6 5.2 copy-start.6
  459.9 5.8 %copy-start.1 = (bf16[1024,512]{0,1:T(8,128)(2,1)S(1)}, bf16[1024,512]{0,1:T(8,128)(2,1)}, u32[]{:S(2)}) copy-start(bf16[1024,512]{0,1:T(8,128)(2,1)} %get-tuple-element.220) | copy-start | bytes 3145732 | tf_op jit(solution)/shard_map/while
  459.9 5.8 %copy-start.5 = (f32[768,4,128]{0,2,1:T(8,128)S(1)}, f32[768,4,128]{0,2,1:T(8,128)}, u32[]{:S(2)}) copy-start(f32[768,4,128]{0,2,1:T(8,128)} %get-tuple-element.238) | copy-start | bytes 4718596 | tf_op jit(solution)/shard_map/while
  468.9 5.2 copy-start.6
  492.2 5.8 %copy-start.1 = (bf16[1024,512]{0,1:T(8,128)(2,1)S(1)}, bf16[1024,512]{0,1:T(8,128)(2,1)}, u32[]{:S(2)}) copy-start(bf16[1024,512]{0,1:T(8,128)(2,1)} %get-tuple-element.220) | copy-start | bytes 3145732 | tf_op jit(solution)/shard_map/while
  492.2 5.8 %copy-start.5 = (f32[768,4,128]{0,2,1:T(8,128)S(1)}, f32[768,4,128]{0,2,1:T(8,128)}, u32[]{:S(2)}) copy-start(f32[768,4,128]{0,2,1:T(8,128)} %get-tuple-element.238) | copy-start | bytes 4718596 | tf_op jit(solution)/shard_map/while
  501.3 5.2 copy-start.6
  509.1 39.8 %copy-start.2 = (bf16[192,2048]{1,0:T(8,128)(2,1)S(1)}, bf16[192,2048]{1,0:T(8,128)(2,1)}, u32[]{:S(2)}) copy-start(bf16[192,2048]{1,0:T(8,128)(2,1)} %param.16) | copy-start | bytes 2359300
  509.1 39.8 %copy-start.8 = (f32[1,1,2048]{2,0,1:T(1,128)S(1)}, f32[1,1,2048]{2,0,1:T(1,128)}, u32[]{:S(2)}) copy-start(f32[1,1,2048]{2,0,1:T(1,128)} %get-tuple-element.125) | copy-start | bytes 24580
Sparse Core Ops, SparseCore 0:
  58.6 25.7 all-gather.3
  86.6 49.0 all-gather.5
  137.9 174.6 all-gather.7
  512.8 36.0 reduce-scatter.1
where the time goes:
time: 559 us; the launch traced here: 558 us
  waiting for transfers between devices  232 us (42%)
  matrix products  145 us (26%)
  local copies, waits for them, and re-layouts  72.2 us (13%)
  other arithmetic  49.9 us (9%)
  blocking collectives  44 us (8%)
  between operations  13.3 us (2%)
    all_gather x1, waiting for transfers between devices, per_device(): portion = lax.all_gather(latent_kv, 'sp', axis=0, tiled=True)  136 us
    dot_general x14, matrix products, absorb(): jnp.einsum('hqk,khd->qhd', raised.astype(jnp.bfloat16), value_rows, prefe...  66.5 us
    dot_general x14, matrix products, absorb(): jnp.einsum('qhd,khd->hqk', queries[:, :, which_map], key_rows[:, :, which...  59 us
    dynamic_slice x12, local copies, waits for them, and re-layouts, absorb_rows(): running, unused = lax.scan(advance, running, (stacked, flag_blocks))  42.2 us
    all_gather x1, waiting for transfers between devices, per_device(): every_context = lax.all_gather(context_kv, 'sp', axis=0, tiled=True)  39.3 us
    reduce_sum x7, other arithmetic, absorb(): weight = weight * faded + jnp.sum(raised, axis=2)  39 us
    psum x1, blocking collectives, per_device(): summed = lax.psum(partials, 'sp')  38.8 us
    reduce_scatter x1, waiting for transfers between devices, per_device(): lax.psum_scatter(jnp.dot(flattened, w_out, preferred_element_type=jnp.flo...  36.2 us
  transfers between devices with their start and end apart: 4, of which 4 were waited for; matrix products, arithmetic and copies ran while one was open for 10% of the time, Pallas kernels for 0%

commit v1 on v0

--- a/solution.py
+++ b/solution.py
@@ -122,7 +122,12 @@
         jnp.zeros((token_count, head_count, 2 * head_dim), jnp.float32),
     )
     initial = first_map + first_map
-    every_context = lax.all_gather(context_kv, "sp", axis=0, tiled=True)
+    ring = [context_kv]
+    for hop in range(7):
+        ring.append(lax.ppermute(ring[-1], "sp", [(dev, (dev + 1) % 8) for dev in range(8)]))
+    every_context = jnp.roll(
+        jnp.concatenate(ring[::-1], axis=0), (lax.axis_index("sp") + 1) * ring[0].shape[0], axis=0
+    )
     running = absorb_rows(
         initial,
         every_context,

time: 559 us -> 545 us (0.975)
  waiting for transfers between devices: 232 us -> 220 us
  matrix products: 145 us -> 138 us
    ppermute x0 -> x7, waiting for transfers between devices: none -> 103 us  [per_device(): lax.ppermute(ring[-1], 'sp', [(dev, (dev + 1) % 8) for dev in range(8)])]
    all_gather x1, waiting for transfers between devices: 136 us -> 52.9 us  [per_device(): portion = lax.all_gather(latent_kv, 'sp', axis=0, tiled=True)]
    all_gather x1 -> x0, waiting for transfers between devices: 39.3 us -> none  [per_device(): every_context = lax.all_gather(context_kv, 'sp', axis=0, tiled=True)]
    dot_general x14, matrix products: 59 us -> 52.9 us  [absorb(): jnp.einsum('qhd,khd->hqk', queries[:, :, which_map], key_rows[:, :, which...]
    unnamed x18 -> x41, local copies, waits for them, and re-layouts: 1.46 us -> 7.2 us
  transfers between devices with their start and end apart: 4 -> 10, of which waited for: 4 -> 10; matrix products, arithmetic and copies ran while one was open for 10% -> 9% of each run, Pallas kernels for 0% -> 0%
where the time goes in v1:
time: 545 us; the launch traced here: 544 us
  waiting for transfers between devices  220 us (40%)
  matrix products  138 us (25%)
  local copies, waits for them, and re-layouts  76.7 us (14%)
  other arithmetic  48.9 us (9%)
  blocking collectives  44 us (8%)
  between operations  13.4 us (2%)
    ppermute x7, waiting for transfers between devices, per_device(): lax.ppermute(ring[-1], 'sp', [(dev, (dev + 1) % 8) for dev in range(8)])  103 us
    dot_general x14, matrix products, absorb(): jnp.einsum('hqk,khd->qhd', raised.astype(jnp.bfloat16), value_rows, prefe...  66.5 us
    dot_general x14, matrix products, absorb(): jnp.einsum('qhd,khd->hqk', queries[:, :, which_map], key_rows[:, :, which...  52.9 us
    all_gather x1, waiting for transfers between devices, per_device(): portion = lax.all_gather(latent_kv, 'sp', axis=0, tiled=True)  52.9 us
    dynamic_slice x12, local copies, waits for them, and re-layouts, absorb_rows(): running, unused = lax.scan(advance, running, (stacked, flag_blocks))  41.9 us
    reduce_sum x7, other arithmetic, absorb(): weight = weight * faded + jnp.sum(raised, axis=2)  39 us
    psum x1, blocking collectives, per_device(): summed = lax.psum(partials, 'sp')  38.8 us
    reduce_scatter x1, waiting for transfers between devices, per_device(): lax.psum_scatter(jnp.dot(flattened, w_out, preferred_element_type=jnp.flo...  37.4 us
  transfers between devices with their start and end apart: 10, of which 10 were waited for; matrix products, arithmetic and copies ran while one was open for 9% of the time, Pallas kernels for 0%

profile of v1, /device:TPU:0, one launch (start us, length us, event | category | flops | bytes accessed | tf_op | source)
XLA Modules:
  0.0 543.6 jit_solution(2605670584975731792)
XLA Ops:
  10.0 38.8 %psum.7 = f32[2,3,512]{2,0,1:T(2,128)S(1)} all-reduce(f32[2,3,512]{2,0,1:T(2,128)S(1)} %pad_maximum_fusion), channel_id=1, replica_groups=mesh['sp'=8,'tp'=4] {'sp'}, use_global_device_ids=true, to_apply=%region_0.1 | all-reduce | flops 3072 | bytes 24576 | tf_op jit(solution)/shard_map/psum | solution.py:101
  48.9 5.2 all_gather.9
  56.1 2.4 fusion.51
  58.5 25.9 %all-gather.3.cloned.1.call-done = bf16[768,2048]{1,0:T(8,128)(2,1)} async-done(((bf16[192,2048]{1,0:T(8,128)(2,1)}), bf16[768,2048]{1,0:T(8,128)(2,1)}) %all-gather.3.cloned.1.call-update) | async-done | bytes 3145744 | tf_op jit(solution)/shard_map/all_gather | solution.py:108
  84.4 8.8 %fusion.44 = bf16[768,1536]{1,0:T(8,128)(2,1)S(1)} fusion(bf16[768,2048]{1,0:T(8,128)(2,1)} %all-gather.3.cloned.1.call-done, bf16[2048,512]{1,0:T(8,128)(2,1)} %param.25, bf16[2048,512]{1,0:T(8,128)(2,1)} %param.24, bf16[2048,512]{1,0:T(8,128)(2,1)} %param.23), kind=kOutput, calls=%fused_computation.56 | convolution fusion | flops 4851892224 | bytes 11796480 | tf_op jit(solution)/shard_map/dot_general | solution.py:107
  96.4 3.0 fusion.57
  100.9 9.8 %collective-permute-done = bf16[128,1024]{1,0:T(8,128)(2,1)S(1)} collective-permute-done((bf16[128,1024]{1,0:T(8,128)(2,1)S(1)}, bf16[128,1024]{1,0:T(8,128)(2,1)S(1)}, u32[]{:S(2)}, u32[]{:S(2)}) %collective-permute-start) | collective-permute-done | bytes 262176 | tf_op jit(solution)/shard_map/ppermute | solution.py:127
  111.2 16.5 %collective-permute-done.1 = bf16[128,1024]{1,0:T(8,128)(2,1)S(1)} collective-permute-done((bf16[128,1024]{1,0:T(8,128)(2,1)S(1)}, bf16[128,1024]{1,0:T(8,128)(2,1)S(1)}, u32[]{:S(2)}, u32[]{:S(2)}) %collective-permute-start.1) | collective-permute-done | bytes 262176 | tf_op jit(solution)/shard_map/ppermute | solution.py:127
  127.7 16.7 %collective-permute-done.2 = bf16[128,1024]{1,0:T(8,128)(2,1)S(1)} collective-permute-done((bf16[128,1024]{1,0:T(8,128)(2,1)S(1)}, bf16[128,1024]{1,0:T(8,128)(2,1)S(1)}, u32[]{:S(2)}, u32[]{:S(2)}) %collective-permute-start.2) | collective-permute-done | bytes 262176 | tf_op jit(solution)/shard_map/ppermute | solution.py:127
  144.4 16.5 %collective-permute-done.3 = bf16[128,1024]{1,0:T(8,128)(2,1)S(1)} collective-permute-done((bf16[128,1024]{1,0:T(8,128)(2,1)S(1)}, bf16[128,1024]{1,0:T(8,128)(2,1)S(1)}, u32[]{:S(2)}, u32[]{:S(2)}) %collective-permute-start.3) | collective-permute-done | bytes 262176 | tf_op jit(solution)/shard_map/ppermute | solution.py:127
  160.9 16.4 %collective-permute-done.4 = bf16[128,1024]{1,0:T(8,128)(2,1)S(1)} collective-permute-done((bf16[128,1024]{1,0:T(8,128)(2,1)S(1)}, bf16[128,1024]{1,0:T(8,128)(2,1)S(1)}, u32[]{:S(2)}, u32[]{:S(2)}) %collective-permute-start.4) | collective-permute-done | bytes 262176 | tf_op jit(solution)/shard_map/ppermute | solution.py:127
  177.9 12.2 %collective-permute-done.5 = bf16[128,1024]{1,0:T(8,128)(2,1)} collective-permute-done((bf16[128,1024]{1,0:T(8,128)(2,1)S(1)}, bf16[128,1024]{1,0:T(8,128)(2,1)}, u32[]{:S(2)}, u32[]{:S(2)}) %collective-permute-start.5) | collective-permute-done | bytes 262176 | tf_op jit(solution)/shard_map/ppermute | solution.py:127
  190.2 15.3 %collective-permute-done.6 = bf16[128,1024]{1,0:T(8,128)(2,1)} collective-permute-done((bf16[128,1024]{1,0:T(8,128)(2,1)}, bf16[128,1024]{1,0:T(8,128)(2,1)}, u32[]{:S(2)}, u32[]{:S(2)}) %collective-permute-start.6) | collective-permute-done | bytes 262176 | tf_op jit(solution)/shard_map/ppermute | solution.py:127
  219.9 3.0 fusion.67
  222.9 6.1 %fusion.25 = (f32[4,768]{1,0:T(4,128)S(1)}, f32[4,768]{1,0:T(4,128)S(1)}, f32[4,768,1024]{2,1,0:T(8,128)}) fusion(f32[4]{0:T(128)S(1)} %copy-done.14, f32[4,768,1024]{2,1,0:T(8,128)S(1)} %fusion.67, bf16[1024,4,2,64]{0,3,2,1:T(8,128)(2,1)S(1)} %bitcast.155, bf16[768,4,2,64]{0,3,2,1:T(8,128)(2,1)S(1)} %bitcast.153), kind=kOutput, calls=%fused_computation.39 | convolution fusion | flops 421521408 | bytes 26108416 | tf_op jit(solution)/shard_map/qhd,khd->hqk/dot_general | solution.py:35
  229.1 8.2 %fusion.29 = (f32[4,768]{1,0:T(4,128)S(1)}, f32[4,768]{1,0:T(4,128)S(1)}) fusion(f32[4,768,1024]{2,1,0:T(8,128)} %get-tuple-element.134, f32[4,768]{1,0:T(4,128)S(1)} %broadcast_maximum_fusion, f32[4]{0:T(128)S(1)} %copy-done.14, f32[4,768]{1,0:T(4,128)S(1)} %broadcast_maximum_fusion.1, f32[4,768,1024]{2,1,0:T(8,128)S(1)} %fusion.67), kind=kLoop, calls=%fused_computation.43 | loop fusion | flops 25159680 | bytes 25214992 | tf_op jit(solution)/shard_map/reduce_sum | solution.py:47
  237.3 8.6 %bitcast_add_fusion.2 = f32[768,4,128]{0,2,1:T(8,128)} fusion(bf16[1024,4,128]{0,2,1:T(8,128)(2,1)S(1)} %bitcast.156, f32[4,768,1024]{2,1,0:T(8,128)} %get-tuple-element.134, f32[4,768]{1,0:T(4,128)S(1)} %broadcast_maximum_fusion, f32[4]{0:T(128)S(1)} %copy-done.14, f32[768,4]{0,1:T(4,128)S(1)} %get-tuple-element.136), kind=kOutput, calls=%fused_computation.67 | convolution fusion | flops 818282496 | bytes 15228944 | tf_op jit(solution)/shard_map/hqk,khd->qhd/dot_general | solution.py:48
  245.8 4.1 bitcast_add_fusion.3
  250.0 52.9 %all-gather.5.cloned.1.call-done = bf16[6144,1024]{1,0:T(8,128)(2,1)} async-done(((bf16[768,1024]{1,0:T(8,128)(2,1)}), bf16[6144,1024]{1,0:T(8,128)(2,1)}) %all-gather.5.cloned.1.call-update) | async-done | bytes 12582928 | tf_op jit(solution)/shard_map/all_gather | solution.py:138
  302.8 188.4 %while.20 = (s32[]{:T(128)}, f32[4,768]{1,0:T(4,128)S(1)}, f32[4,768]{1,0:T(4,128)S(1)}, f32[768,4,128]{0,2,1:T(8,128)}, f32[4,768]{1,0:T(4,128)S(1)}, /*index=5...) while((s32[]{:T(128)}, f32[4,768]{1,0:T(4,128)S(1)}, ...), condition=%wide.region_12.13_spmd, body=%wide.region_7.12_spmd.sunk | while | flops 2486716416 | bytes 131203896 | solution.py:69
  302.8 3.1 constant_dynamic-slice_fusion.3
  305.9 3.9 copy.54
  309.8 2.8 fusion.114
  314.5 5.5 %bitcast_reduce_fusion.3 = (f32[4,768]{1,0:T(4,128)S(1)}, f32[4,768]{1,0:T(4,128)S(1)}, f32[4,1024,768]{2,1,0:T(8,128)S(1)}) fusion(f32[4]{0:T(128)S(1)} %broadcast_multiply_fusion.2, f32[4,1024,768]{2,1,0:T(8,128)S(1)} %fusion.115, bf16[768,4,2,64]{0,3,1,2:T(8,128)(2,1)} %get-tuple-element.254, bf16[1024,4,2,64]{0,3,2,1:T(8,128)(2,1)S(1)} %bitcast.147), kind=kOutput, calls=%fused_computation.1.clone.1 | convolution fusion | flops 421521408 | bytes 26108416 | tf_op jit(solution)/shard_map/while/body/eval_jaxpr/qhd,khd->hqk/dot_general | solution.py:35
  320.0 5.8 %bitcast_add_fusion.7 = f32[768,4,128]{0,2,1:T(8,128)} fusion(f32[768,4,128]{0,2,1:T(8,128)} %get-tuple-element.241, bf16[1024,4,128]{0,2,1:T(8,128)(2,1)} %bitcast.148, f32[4,1024,768]{2,1,0:T(8,128)S(1)} %get-tuple-element.214, f32[4,768]{1,0:T(4,128)S(1)} %get-tuple-element.250, f32[4]{0:T(128)S(1)} %broadcast_multiply_fusion.2, ...), kind=kOutput, calls=%fused_computation.14.clone.1 | convolution fusion | flops 818675712 | bytes 16801808 | tf_op jit(solution)/shard_map/while/body/eval_jaxpr/hqk,khd->qhd/dot_general | solution.py:48
  325.8 3.2 bitcast_add_fusion.6
  329.0 5.1 fusion.118
  334.2 3.1 constant_dynamic-slice_fusion.3
  337.3 3.9 copy.54
  341.2 2.8 fusion.114
  345.9 5.5 %bitcast_reduce_fusion.3 = (f32[4,768]{1,0:T(4,128)S(1)}, f32[4,768]{1,0:T(4,128)S(1)}, f32[4,1024,768]{2,1,0:T(8,128)S(1)}) fusion(f32[4]{0:T(128)S(1)} %broadcast_multiply_fusion.2, f32[4,1024,768]{2,1,0:T(8,128)S(1)} %fusion.115, bf16[768,4,2,64]{0,3,1,2:T(8,128)(2,1)} %get-tuple-element.254, bf16[1024,4,2,64]{0,3,2,1:T(8,128)(2,1)S(1)} %bitcast.147), kind=kOutput, calls=%fused_computation.1.clone.1 | convolution fusion | flops 421521408 | bytes 26108416 | tf_op jit(solution)/shard_map/while/body/eval_jaxpr/qhd,khd->hqk/dot_general | solution.py:35
  351.4 5.8 %bitcast_add_fusion.7 = f32[768,4,128]{0,2,1:T(8,128)} fusion(f32[768,4,128]{0,2,1:T(8,128)} %get-tuple-element.241, bf16[1024,4,128]{0,2,1:T(8,128)(2,1)} %bitcast.148, f32[4,1024,768]{2,1,0:T(8,128)S(1)} %get-tuple-element.214, f32[4,768]{1,0:T(4,128)S(1)} %get-tuple-element.250, f32[4]{0:T(128)S(1)} %broadcast_multiply_fusion.2, ...), kind=kOutput, calls=%fused_computation.14.clone.1 | convolution fusion | flops 818675712 | bytes 16801808 | tf_op jit(solution)/shard_map/while/body/eval_jaxpr/hqk,khd->qhd/dot_general | solution.py:48
  357.2 3.2 bitcast_add_fusion.6
  360.4 5.1 fusion.118
  365.6 3.1 constant_dynamic-slice_fusion.3
  368.7 3.9 copy.54
  372.6 2.8 fusion.114
  377.3 5.5 %bitcast_reduce_fusion.3 = (f32[4,768]{1,0:T(4,128)S(1)}, f32[4,768]{1,0:T(4,128)S(1)}, f32[4,1024,768]{2,1,0:T(8,128)S(1)}) fusion(f32[4]{0:T(128)S(1)} %broadcast_multiply_fusion.2, f32[4,1024,768]{2,1,0:T(8,128)S(1)} %fusion.115, bf16[768,4,2,64]{0,3,1,2:T(8,128)(2,1)} %get-tuple-element.254, bf16[1024,4,2,64]{0,3,2,1:T(8,128)(2,1)S(1)} %bitcast.147), kind=kOutput, calls=%fused_computation.1.clone.1 | convolution fusion | flops 421521408 | bytes 26108416 | tf_op jit(solution)/shard_map/while/body/eval_jaxpr/qhd,khd->hqk/dot_general | solution.py:35
  382.8 5.8 %bitcast_add_fusion.7 = f32[768,4,128]{0,2,1:T(8,128)} fusion(f32[768,4,128]{0,2,1:T(8,128)} %get-tuple-element.241, bf16[1024,4,128]{0,2,1:T(8,128)(2,1)} %bitcast.148, f32[4,1024,768]{2,1,0:T(8,128)S(1)} %get-tuple-element.214, f32[4,768]{1,0:T(4,128)S(1)} %get-tuple-element.250, f32[4]{0:T(128)S(1)} %broadcast_multiply_fusion.2, ...), kind=kOutput, calls=%fused_computation.14.clone.1 | convolution fusion | flops 818675712 | bytes 16801808 | tf_op jit(solution)/shard_map/while/body/eval_jaxpr/hqk,khd->qhd/dot_general | solution.py:48
  388.6 3.2 bitcast_add_fusion.6
  391.8 5.1 fusion.118
  397.0 3.1 constant_dynamic-slice_fusion.3
  400.1 3.9 copy.54
  404.0 2.8 fusion.114
  408.7 5.5 %bitcast_reduce_fusion.3 = (f32[4,768]{1,0:T(4,128)S(1)}, f32[4,768]{1,0:T(4,128)S(1)}, f32[4,1024,768]{2,1,0:T(8,128)S(1)}) fusion(f32[4]{0:T(128)S(1)} %broadcast_multiply_fusion.2, f32[4,1024,768]{2,1,0:T(8,128)S(1)} %fusion.115, bf16[768,4,2,64]{0,3,1,2:T(8,128)(2,1)} %get-tuple-element.254, bf16[1024,4,2,64]{0,3,2,1:T(8,128)(2,1)S(1)} %bitcast.147), kind=kOutput, calls=%fused_computation.1.clone.1 | convolution fusion | flops 421521408 | bytes 26108416 | tf_op jit(solution)/shard_map/while/body/eval_jaxpr/qhd,khd->hqk/dot_general | solution.py:35
  414.2 5.8 %bitcast_add_fusion.7 = f32[768,4,128]{0,2,1:T(8,128)} fusion(f32[768,4,128]{0,2,1:T(8,128)} %get-tuple-element.241, bf16[1024,4,128]{0,2,1:T(8,128)(2,1)} %bitcast.148, f32[4,1024,768]{2,1,0:T(8,128)S(1)} %get-tuple-element.214, f32[4,768]{1,0:T(4,128)S(1)} %get-tuple-element.250, f32[4]{0:T(128)S(1)} %broadcast_multiply_fusion.2, ...), kind=kOutput, calls=%fused_computation.14.clone.1 | convolution fusion | flops 818675712 | bytes 16801808 | tf_op jit(solution)/shard_map/while/body/eval_jaxpr/hqk,khd->qhd/dot_general | solution.py:48
  420.0 3.2 bitcast_add_fusion.6
  423.2 5.1 fusion.118
  428.4 3.1 constant_dynamic-slice_fusion.3
  431.5 3.9 copy.54
  435.4 2.8 fusion.114
  440.0 5.5 %bitcast_reduce_fusion.3 = (f32[4,768]{1,0:T(4,128)S(1)}, f32[4,768]{1,0:T(4,128)S(1)}, f32[4,1024,768]{2,1,0:T(8,128)S(1)}) fusion(f32[4]{0:T(128)S(1)} %broadcast_multiply_fusion.2, f32[4,1024,768]{2,1,0:T(8,128)S(1)} %fusion.115, bf16[768,4,2,64]{0,3,1,2:T(8,128)(2,1)} %get-tuple-element.254, bf16[1024,4,2,64]{0,3,2,1:T(8,128)(2,1)S(1)} %bitcast.147), kind=kOutput, calls=%fused_computation.1.clone.1 | convolution fusion | flops 421521408 | bytes 26108416 | tf_op jit(solution)/shard_map/while/body/eval_jaxpr/qhd,khd->hqk/dot_general | solution.py:35
  445.6 5.8 %bitcast_add_fusion.7 = f32[768,4,128]{0,2,1:T(8,128)} fusion(f32[768,4,128]{0,2,1:T(8,128)} %get-tuple-element.241, bf16[1024,4,128]{0,2,1:T(8,128)(2,1)} %bitcast.148, f32[4,1024,768]{2,1,0:T(8,128)S(1)} %get-tuple-element.214, f32[4,768]{1,0:T(4,128)S(1)} %get-tuple-element.250, f32[4]{0:T(128)S(1)} %broadcast_multiply_fusion.2, ...), kind=kOutput, calls=%fused_computation.14.clone.1 | convolution fusion | flops 818675712 | bytes 16801808 | tf_op jit(solution)/shard_map/while/body/eval_jaxpr/hqk,khd->qhd/dot_general | solution.py:48
  451.4 3.2 bitcast_add_fusion.6
  454.6 5.1 fusion.118
  459.8 3.1 constant_dynamic-slice_fusion.3
  462.9 3.9 copy.54
  466.8 2.8 fusion.114
  471.4 5.5 %bitcast_reduce_fusion.3 = (f32[4,768]{1,0:T(4,128)S(1)}, f32[4,768]{1,0:T(4,128)S(1)}, f32[4,1024,768]{2,1,0:T(8,128)S(1)}) fusion(f32[4]{0:T(128)S(1)} %broadcast_multiply_fusion.2, f32[4,1024,768]{2,1,0:T(8,128)S(1)} %fusion.115, bf16[768,4,2,64]{0,3,1,2:T(8,128)(2,1)} %get-tuple-element.254, bf16[1024,4,2,64]{0,3,2,1:T(8,128)(2,1)S(1)} %bitcast.147), kind=kOutput, calls=%fused_computation.1.clone.1 | convolution fusion | flops 421521408 | bytes 26108416 | tf_op jit(solution)/shard_map/while/body/eval_jaxpr/qhd,khd->hqk/dot_general | solution.py:35
  477.0 5.8 %bitcast_add_fusion.7 = f32[768,4,128]{0,2,1:T(8,128)} fusion(f32[768,4,128]{0,2,1:T(8,128)} %get-tuple-element.241, bf16[1024,4,128]{0,2,1:T(8,128)(2,1)} %bitcast.148, f32[4,1024,768]{2,1,0:T(8,128)S(1)} %get-tuple-element.214, f32[4,768]{1,0:T(4,128)S(1)} %get-tuple-element.250, f32[4]{0:T(128)S(1)} %broadcast_multiply_fusion.2, ...), kind=kOutput, calls=%fused_computation.14.clone.1 | convolution fusion | flops 818675712 | bytes 16801808 | tf_op jit(solution)/shard_map/while/body/eval_jaxpr/hqk,khd->qhd/dot_general | solution.py:48
  482.8 3.2 bitcast_add_fusion.6
  486.0 5.1 fusion.118
  493.9 3.5 convolution_convert_fusion
  497.4 37.4 %reduce-scatter.2.cloned.1.call-done = bf16[192,2048]{1,0:T(8,128)(2,1)} async-done(((bf16[768,2048]{1,0:T(8,128)(2,1)}), bf16[192,2048]{1,0:T(8,128)(2,1)}) %reduce-scatter.2.cloned.1.call-update) | async-done | bytes 786448 | tf_op jit(solution)/shard_map/reduce_scatter | solution.py:148
  (168 shorter events, 42.2 us)
Async XLA Ops:
  6.5 487.3 %copy-start = (bf16[512,2048]{1,0:T(8,128)(2,1)S(1)}, bf16[512,2048]{1,0:T(8,128)(2,1)}, u32[]{:S(2)}) copy-start(bf16[512,2048]{1,0:T(8,128)(2,1)} %param.26) | copy-start | bytes 6291460
  6.5 77.9 %all-gather.3.cloned.1.call-start = ((), (), s32[]{:S(2)}) async-start(), calls=%async_computation.1 | async-start | bytes 3932160 | tf_op jit(solution)/shard_map/all_gather | solution.py:108
  58.5 244.3 %all-gather.5.cloned.1.call-start = ((), (), s32[]{:S(2)}) async-start(), calls=%async_computation.2 | async-start | bytes 14155776 | tf_op jit(solution)/shard_map/all_gather | solution.py:138
  93.2 1.4 copy-start.5
  94.7 1.5 copy-start.11
  94.7 1.7 copy-start.13
  96.1 438.6 %reduce-scatter.2.cloned.1.call-start = ((), (), s32[]{:S(2)}) async-start(), calls=%async_computation.3 | async-start | bytes 3932160 | tf_op jit(solution)/shard_map/reduce_scatter | solution.py:148
  99.4 11.3 %collective-permute-start = (bf16[128,1024]{1,0:T(8,128)(2,1)S(1)}, bf16[128,1024]{1,0:T(8,128)(2,1)S(1)}, u32[]{:S(2)}, u32[]{:S(2)}) collective-permute-start(bf16[128,1024]{1,0:T(8,128)(2,1)S(1)} %fusion.57), channel_id=1, source_target_pairs={{0,4},{4,8},{8,12},{12,16},{16,20},{20,24},{24,28},{28,0},{1,5},{5... | collective-permute-start | bytes 786440 | tf_op jit(solution)/shard_map/ppermute | solution.py:127
  110.7 17.0 %collective-permute-start.1 = (bf16[128,1024]{1,0:T(8,128)(2,1)S(1)}, bf16[128,1024]{1,0:T(8,128)(2,1)S(1)}, u32[]{:S(2)}, u32[]{:S(2)}) collective-permute-start(bf16[128,1024]{1,0:T(8,128)(2,1)S(1)} %collective-permute-done), channel_id=1, source_target_pairs={{0,4},{4,8},{8,12},{12,16},{16,20},{20,24},{24,28},{28,0},{1,5},{5... | collective-permute-start | bytes 786440 | tf_op jit(solution)/shard_map/ppermute | solution.py:127
  127.7 16.7 %collective-permute-start.2 = (bf16[128,1024]{1,0:T(8,128)(2,1)S(1)}, bf16[128,1024]{1,0:T(8,128)(2,1)S(1)}, u32[]{:S(2)}, u32[]{:S(2)}) collective-permute-start(bf16[128,1024]{1,0:T(8,128)(2,1)S(1)} %collective-permute-done.1), channel_id=1, source_target_pairs={{0,4},{4,8},{8,12},{12,16},{16,20},{20,24},{24,28},{28,0},{1,5},{5... | collective-permute-start | bytes 786440 | tf_op jit(solution)/shard_map/ppermute | solution.py:127
  144.4 16.5 %collective-permute-start.3 = (bf16[128,1024]{1,0:T(8,128)(2,1)S(1)}, bf16[128,1024]{1,0:T(8,128)(2,1)S(1)}, u32[]{:S(2)}, u32[]{:S(2)}) collective-permute-start(bf16[128,1024]{1,0:T(8,128)(2,1)S(1)} %collective-permute-done.2), channel_id=1, source_target_pairs={{0,4},{4,8},{8,12},{12,16},{16,20},{20,24},{24,28},{28,0},{1,5},{5... | collective-permute-start | bytes 786440 | tf_op jit(solution)/shard_map/ppermute | solution.py:127
  160.9 16.4 %collective-permute-start.4 = (bf16[128,1024]{1,0:T(8,128)(2,1)S(1)}, bf16[128,1024]{1,0:T(8,128)(2,1)S(1)}, u32[]{:S(2)}, u32[]{:S(2)}) collective-permute-start(bf16[128,1024]{1,0:T(8,128)(2,1)S(1)} %collective-permute-done.3), channel_id=1, source_target_pairs={{0,4},{4,8},{8,12},{12,16},{16,20},{20,24},{24,28},{28,0},{1,5},{5... | collective-permute-start | bytes 786440 | tf_op jit(solution)/shard_map/ppermute | solution.py:127
  177.2 0.7 copy-start.9
  177.9 12.2 %collective-permute-start.5 = (bf16[128,1024]{1,0:T(8,128)(2,1)S(1)}, bf16[128,1024]{1,0:T(8,128)(2,1)}, u32[]{:S(2)}, u32[]{:S(2)}) collective-permute-start(bf16[128,1024]{1,0:T(8,128)(2,1)S(1)} %collective-permute-done.4), channel_id=1, source_target_pairs={{0,4},{4,8},{8,12},{12,16},{16,20},{20,24},{24,28},{28,0},{1,5},{5... | collective-permute-start | bytes 786440 | tf_op jit(solution)/shard_map/ppermute | solution.py:127
  190.2 15.3 %collective-permute-start.6 = (bf16[128,1024]{1,0:T(8,128)(2,1)}, bf16[128,1024]{1,0:T(8,128)(2,1)}, u32[]{:S(2)}, u32[]{:S(2)}) collective-permute-start(bf16[128,1024]{1,0:T(8,128)(2,1)} %collective-permute-done.5), channel_id=1, source_target_pairs={{0,4},{4,8},{8,12},{12,16},{16,20},{20,24},{24,28},{28,0},{1,5},{5... | collective-permute-start | bytes 786440 | tf_op jit(solution)/shard_map/ppermute | solution.py:127
  190.2 20.3 %copy-start.10 = (bf16[128,1024]{1,0:T(8,128)(2,1)S(1)}, bf16[128,1024]{1,0:T(8,128)(2,1)}, u32[]{:S(2)}) copy-start(bf16[128,1024]{1,0:T(8,128)(2,1)} %copy-done.9) | copy-start | bytes 786436
  219.9 3.0 copy-start.4
  219.9 3.0 copy-start.14
  229.1 8.2 %copy-start.8 = (bf16[1024,512]{0,1:T(8,128)(2,1)S(1)}, bf16[1024,512]{0,1:T(8,128)(2,1)}, u32[]{:S(2)}) copy-start(bf16[1024,512]{0,1:T(8,128)(2,1)} %copy.41) | copy-start | bytes 3145732
  302.8 188.4 %copy-start.15 = (f32[4]{0:T(128)S(1)}, f32[4]{0:T(128)}, u32[]{:S(2)}) copy-start(f32[4]{0:T(128)} %param.27) | copy-start | bytes 52
  309.8 2.8 copy-start.1
  320.0 5.8 %copy-start.2 = (bf16[1024,512]{0,1:T(8,128)(2,1)S(1)}, bf16[1024,512]{0,1:T(8,128)(2,1)}, u32[]{:S(2)}) copy-start(bf16[1024,512]{0,1:T(8,128)(2,1)} %get-tuple-element.220) | copy-start | bytes 3145732 | tf_op jit(solution)/shard_map/while
  320.0 5.8 %copy-start.6 = (f32[768,4,128]{0,2,1:T(8,128)S(1)}, f32[768,4,128]{0,2,1:T(8,128)}, u32[]{:S(2)}) copy-start(f32[768,4,128]{0,2,1:T(8,128)} %get-tuple-element.238) | copy-start | bytes 4718596 | tf_op jit(solution)/shard_map/while
  329.0 5.2 copy-start.7
  341.2 2.8 copy-start.1
  351.4 5.8 %copy-start.2 = (bf16[1024,512]{0,1:T(8,128)(2,1)S(1)}, bf16[1024,512]{0,1:T(8,128)(2,1)}, u32[]{:S(2)}) copy-start(bf16[1024,512]{0,1:T(8,128)(2,1)} %get-tuple-element.220) | copy-start | bytes 3145732 | tf_op jit(solution)/shard_map/while
  351.4 5.8 %copy-start.6 = (f32[768,4,128]{0,2,1:T(8,128)S(1)}, f32[768,4,128]{0,2,1:T(8,128)}, u32[]{:S(2)}) copy-start(f32[768,4,128]{0,2,1:T(8,128)} %get-tuple-element.238) | copy-start | bytes 4718596 | tf_op jit(solution)/shard_map/while
  360.4 5.2 copy-start.7
  372.6 2.8 copy-start.1
  382.8 5.8 %copy-start.2 = (bf16[1024,512]{0,1:T(8,128)(2,1)S(1)}, bf16[1024,512]{0,1:T(8,128)(2,1)}, u32[]{:S(2)}) copy-start(bf16[1024,512]{0,1:T(8,128)(2,1)} %get-tuple-element.220) | copy-start | bytes 3145732 | tf_op jit(solution)/shard_map/while
  382.8 5.8 %copy-start.6 = (f32[768,4,128]{0,2,1:T(8,128)S(1)}, f32[768,4,128]{0,2,1:T(8,128)}, u32[]{:S(2)}) copy-start(f32[768,4,128]{0,2,1:T(8,128)} %get-tuple-element.238) | copy-start | bytes 4718596 | tf_op jit(solution)/shard_map/while
  391.8 5.2 copy-start.7
  404.0 2.8 copy-start.1
  414.1 5.8 %copy-start.2 = (bf16[1024,512]{0,1:T(8,128)(2,1)S(1)}, bf16[1024,512]{0,1:T(8,128)(2,1)}, u32[]{:S(2)}) copy-start(bf16[1024,512]{0,1:T(8,128)(2,1)} %get-tuple-element.220) | copy-start | bytes 3145732 | tf_op jit(solution)/shard_map/while
  414.2 5.8 %copy-start.6 = (f32[768,4,128]{0,2,1:T(8,128)S(1)}, f32[768,4,128]{0,2,1:T(8,128)}, u32[]{:S(2)}) copy-start(f32[768,4,128]{0,2,1:T(8,128)} %get-tuple-element.238) | copy-start | bytes 4718596 | tf_op jit(solution)/shard_map/while
  423.2 5.2 copy-start.7
  435.4 2.8 copy-start.1
  445.5 5.8 %copy-start.2 = (bf16[1024,512]{0,1:T(8,128)(2,1)S(1)}, bf16[1024,512]{0,1:T(8,128)(2,1)}, u32[]{:S(2)}) copy-start(bf16[1024,512]{0,1:T(8,128)(2,1)} %get-tuple-element.220) | copy-start | bytes 3145732 | tf_op jit(solution)/shard_map/while
  445.6 5.8 %copy-start.6 = (f32[768,4,128]{0,2,1:T(8,128)S(1)}, f32[768,4,128]{0,2,1:T(8,128)}, u32[]{:S(2)}) copy-start(f32[768,4,128]{0,2,1:T(8,128)} %get-tuple-element.238) | copy-start | bytes 4718596 | tf_op jit(solution)/shard_map/while
  454.6 5.2 copy-start.7
  466.8 2.8 copy-start.1
  476.9 5.8 %copy-start.2 = (bf16[1024,512]{0,1:T(8,128)(2,1)S(1)}, bf16[1024,512]{0,1:T(8,128)(2,1)}, u32[]{:S(2)}) copy-start(bf16[1024,512]{0,1:T(8,128)(2,1)} %get-tuple-element.220) | copy-start | bytes 3145732 | tf_op jit(solution)/shard_map/while
  476.9 5.8 %copy-start.6 = (f32[768,4,128]{0,2,1:T(8,128)S(1)}, f32[768,4,128]{0,2,1:T(8,128)}, u32[]{:S(2)}) copy-start(f32[768,4,128]{0,2,1:T(8,128)} %get-tuple-element.238) | copy-start | bytes 4718596 | tf_op jit(solution)/shard_map/while
  486.0 5.2 copy-start.7
  491.2 2.3 copy-start.16
  493.8 40.9 %copy-start.3 = (bf16[192,2048]{1,0:T(8,128)(2,1)S(1)}, bf16[192,2048]{1,0:T(8,128)(2,1)}, u32[]{:S(2)}) copy-start(bf16[192,2048]{1,0:T(8,128)(2,1)} %param.16) | copy-start | bytes 2359300
  493.9 40.9 %copy-start.12 = (f32[1,1,2048]{2,0,1:T(1,128)S(1)}, f32[1,1,2048]{2,0,1:T(1,128)}, u32[]{:S(2)}) copy-start(f32[1,1,2048]{2,0,1:T(1,128)} %get-tuple-element.125) | copy-start | bytes 24580
Sparse Core Ops, SparseCore 0:
  58.6 25.7 all-gather.2
  96.3 206.5 all-gather.4
  497.5 37.2 reduce-scatter.1
